TPU v7x, 32 devices: a whole 2x2x4 slice. The times are simulated.
32 devices in a mesh: sp: 4 (over z), fs: 4 (over y, x), tp: 2 (over core).
Axes of the slice: x: 2, y: 2, z: 4, core: 2. Of those that a mesh axis runs over, the one named last changes fastest.
Arguments:
- tokens: bfloat16 [4, 8192, 2048], P('fs', 'sp'), may hold values from -21 to 21
- norm_gain: float32 [2048], replicated, may hold values from 0.1 to 1.9
- w_query: bfloat16 [2048, 1024], P(None, 'tp'), may hold values from -0.125 to 0.125
- w_key: bfloat16 [2048, 256], P(None, 'tp'), may hold values from -0.125 to 0.125
- w_value: bfloat16 [2048, 256], P(None, 'tp'), may hold values from -0.125 to 0.125
- w_pool: bfloat16 [2048, 1024], P(None, 'tp'), may hold values from -0.125 to 0.125
- w_group: bfloat16 [4, 256, 256], P('tp'), may hold values from -0.375 to 0.375
- w_out: bfloat16 [2048, 2048], replicated, may hold values from -0.125 to 0.125
- sinks: float32 [16], P('tp'), may hold values from -1 to 260
Outputs:
- mixed: bfloat16 [4, 8192, 2048], P('fs', ('sp', 'tp'))
- log_sums: float32 [4, 16, 8192], P('fs', 'tp', 'sp')
All inputs are finite; a program needn't handle non-finite values.
Results may differ from a plain program's by a relative error of at most 0.009.
Values may be sent and summed in bfloat16 or wider, within the bound.
A program may use at most 192 MiB of HBM per device.

v0:
```python
import functools

import jax
import jax.numpy as jnp
from jax import lax
from jax.experimental import pallas as pl
from jax.experimental.pallas import tpu as pltpu
from jax.sharding import PartitionSpec as P

HEAD_SIZE = 64
GDIM = 256
WINDOW = 128
LN_EPS = 1e-05
VMEM = 63 * 2**20
MESH = pl.DeviceIdType.MESH
BF = jnp.bfloat16
F32 = jnp.float32
NEG = -1e30


def dot(a, b, dims=((1,), (0,))):
    return lax.dot_general(a, b, (dims, ((), ())), preferred_element_type=F32)


def normalize(tok, gain, normed):
    width = tok.shape[1]

    def chunk(j):
        rows = slice(j * 64, (j + 1) * 64)
        x = tok[rows, :].astype(F32)
        centered = x - jnp.sum(x, axis=-1, keepdims=True) * (1.0 / width)
        variance = jnp.sum(centered * centered, axis=-1, keepdims=True) * (1.0 / width)
        normed[rows, :] = (centered * lax.rsqrt(variance + LN_EPS) * gain[...]).astype(BF)

    return [functools.partial(chunk, j) for j in range(tok.shape[0] // 64)]


def multiply(normed, wq, wk, wv, wp, q, kd, vt, pool, bsum, total, step):
    def do_q():
        q[...] = (dot(normed[...], wq[...]) * HEAD_SIZE**-0.5).astype(BF)

    def do_k():
        k = dot(normed[...], wk[...])
        rolled = pltpu.roll(k, HEAD_SIZE, 1)
        low = lax.broadcasted_iota(jnp.int32, k.shape, 1) < HEAD_SIZE
        kd[:, :WINDOW] = jnp.where(low, k, rolled).astype(BF)
        kd[:, WINDOW:] = jnp.where(low, rolled, k).astype(BF)

    def do_v():
        vt[...] = dot(normed[...], wv[...]).T.astype(BF)

    def do_p():
        p = dot(normed[...], wp[...]).astype(BF)
        pool[...] = p
        pf = p.astype(F32)
        sums = [
            jnp.sum(pf[b * WINDOW : (b + 1) * WINDOW], axis=0, keepdims=True)
            for b in range(p.shape[0] // WINDOW)
        ]
        tile_sum = functools.reduce(lambda a, b: a + b, sums)
        pad = jnp.zeros((8 - len(sums), pool.shape[1]), F32)
        bsum[0] = jnp.concatenate(sums + [pad], axis=0)
        total[...] = jnp.where(step > 1, total[...], 0.0) + tile_sum

    return [do_q, do_k, do_v, do_p]


def project_kernel(steps, tok, gain, wq, wk, wv, wp, q, kd, vt, pool, bsum, total, even, odd):
    step = pl.program_id(0)
    rest = (wq, wk, wv, wp, q, kd, vt, pool, bsum, total, step)

    @pl.when(step == 0)
    def _():
        for f in normalize(tok, gain, even):
            f()

    for parity in range(2):
        here, before = (even, odd) if parity == 0 else (odd, even)

        @pl.when((step > 0) & (step < steps) & (step % 2 == parity))
        def _():
            norms, mults = normalize(tok, gain, here), multiply(before, *rest)
            for n, m in zip(norms, mults):
                n()
                m()

    @pl.when(step == steps)
    def _():
        for f in multiply(odd if steps % 2 == 0 else even, *rest):
            f()


def project(tokens, gain, wq, wk, wv, wp):
    length, width = tokens.shape
    tile = 256
    steps = length // tile
    late = lambda i: jnp.maximum(i - 1, 0)
    qw, kw, pw = wq.shape[1], wk.shape[1], wp.shape[1]
    whole = lambda a: pl.BlockSpec(a.shape, lambda i: (0, 0), pipeline_mode=pl.Buffered(1))
    return pl.pallas_call(
        functools.partial(project_kernel, steps),
        grid=(steps + 1,),
        in_specs=[
            pl.BlockSpec((tile, width), lambda i: (jnp.minimum(i, steps - 1), 0)),
            whole(gain), whole(wq), whole(wk), whole(wv), whole(wp),
        ],
        out_specs=[
            pl.BlockSpec((tile, qw), lambda i: (late(i), 0)),
            pl.BlockSpec((tile, 2 * kw), lambda i: (late(i), 0)),
            pl.BlockSpec((kw, tile), lambda i: (0, late(i))),
            pl.BlockSpec((tile, pw), lambda i: (late(i), 0)),
            pl.BlockSpec((1, 8, pw), lambda i: (late(i), 0, 0)),
            pl.BlockSpec((1, pw), lambda i: (0, 0)),
        ],
        out_shape=[
            jax.ShapeDtypeStruct((length, qw), BF),
            jax.ShapeDtypeStruct((length, 2 * kw), BF),
            jax.ShapeDtypeStruct((kw, length), BF),
            jax.ShapeDtypeStruct((length, pw), BF),
            jax.ShapeDtypeStruct((steps, 8, pw), F32),
            jax.ShapeDtypeStruct((1, pw), F32),
        ],
        scratch_shapes=[pltpu.VMEM((tile, width), BF)] * 2,
        compiler_params=pltpu.CompilerParams(
            dimension_semantics=("arbitrary",), vmem_limit_bytes=VMEM
        ),
        cost_estimate=pl.CostEstimate(
            flops=2 * length * width * (qw + 2 * kw + pw),
            bytes_accessed=2 * length * width, transcendentals=0,
        ),
        name="project",
    )(tokens, gain, wq, wk, wv, wp)


def mix_kernel(
    mine, scal, q, kc, kp, vc, vp, pc, pp, khalo, vhalo, phalo, totals, bsum, wg, sinks, *outs
):
    out, logs = outs[-2:]
    step = pl.program_id(0)
    tp, sp, steps = scal[0], scal[1], scal[2]
    half = tp if mine else 1 - tp
    earlier = jnp.sum(totals[...], axis=0)
    first_step = half * pl.num_programs(0) + step
    tile = q.shape[0]
    at_start = first_step == 0
    keys = jnp.concatenate([jnp.where(at_start, khalo[...], kp[...]), kc[...]], axis=0)
    vals = jnp.concatenate([jnp.where(at_start, vhalo[...], vp[...]), vc[...]], axis=1)
    padded = jnp.concatenate(
        [jnp.zeros((WINDOW - phalo.shape[0], phalo.shape[1]), BF), phalo[...]], axis=0
    )
    rows = jnp.concatenate([jnp.where(at_start, padded, pp[...]), pc[...]], axis=0)
    lane = lax.broadcasted_iota(jnp.int32, (WINDOW, WINDOW), 1)
    low = (lane < HEAD_SIZE).astype(F32).astype(BF)
    high = (lane >= HEAD_SIZE).astype(F32).astype(BF)
    heads = 4
    key_id = lax.broadcasted_iota(jnp.int32, (WINDOW, heads * WINDOW), 0)
    query_id = lax.broadcasted_iota(jnp.int32, (WINDOW, heads * WINDOW), 1) % WINDOW
    seen = key_id <= query_id
    seen_f = seen.astype(F32).astype(BF)
    past_f = (key_id > query_id).astype(F32).astype(BF)
    nopast = jnp.logical_and(at_start, sp == 0)
    groups = wg.shape[0]
    drow = lax.broadcasted_iota(jnp.int32, (WINDOW, 2 * WINDOW), 0)
    dist = drow + WINDOW - lax.broadcasted_iota(jnp.int32, (WINDOW, 2 * WINDOW), 1)
    prefix = jnp.logical_and(dist >= 0, dist <= drow).astype(F32).astype(BF)
    blocks_per_sum = scal[3]
    sum_id = lax.broadcasted_iota(jnp.int32, bsum.shape, 0) * blocks_per_sum + (
        lax.broadcasted_iota(jnp.int32, bsum.shape, 1)
    )
    kvs = kc.shape[1] // WINDOW
    nblocks = tile // WINDOW
    sink_rows = [
        jnp.concatenate(
            [jnp.full((1, WINDOW), sinks[kv * heads + h], F32) for h in range(heads)], axis=1
        )
        for kv in range(kvs)
    ]

    def score(b, kv):
        parts = []
        for pair in range(2):
            c = (kv * 2 + pair) * WINDOW
            qp = q[b * WINDOW : (b + 1) * WINDOW, c : c + WINDOW]
            parts += [qp * low, qp * high]
        wr = slice(b * WINDOW, (b + 2) * WINDOW)
        return dot(
            keys[wr, kv * WINDOW : (kv + 1) * WINDOW], jnp.concatenate(parts, axis=0), ((1,), (1,))
        )

    def attend(b, kv, scores):
        br = slice(b * WINDOW, (b + 1) * WINDOW)
        past = scores[:WINDOW]
        if b == 0:
            past = past + jnp.where(nopast, F32(NEG), F32(0))
        picked = jnp.where(seen, scores[WINDOW:], past)
        sink = sink_rows[kv]
        row_max = jnp.maximum(jnp.max(picked, axis=0, keepdims=True), sink)
        weights = jnp.exp(picked - row_max)
        weight_sum = jnp.sum(weights, axis=0, keepdims=True) + jnp.exp(sink - row_max)
        log_row = row_max + jnp.log(weight_sum)
        for h in range(heads):
            logs[kv * heads + h : kv * heads + h + 1, br] = log_row[:, h * WINDOW : (h + 1) * WINDOW]
        wb = weights.astype(BF)
        stacked = jnp.concatenate([wb * past_f, wb * seen_f], axis=0)
        return stacked, 1.0 / weight_sum

    def collect(b, kv, stacked, scale):
        wr = slice(b * WINDOW, (b + 2) * WINDOW)
        o = dot(vals[kv * HEAD_SIZE : (kv + 1) * HEAD_SIZE, wr], stacked) * scale
        o = jnp.concatenate([o[:, h * WINDOW : (h + 1) * WINDOW] for h in range(heads)], axis=0)
        width = heads * HEAD_SIZE
        out[1, b * WINDOW : (b + 1) * WINDOW, kv * width : (kv + 1) * width] = o.astype(BF).T

    sum_row = lax.broadcasted_iota(jnp.int32, bsum.shape, 1)

    def pool_block(b, g):
        br = slice(b * WINDOW, (b + 1) * WINDOW)
        wr = slice(b * WINDOW, (b + 2) * WINDOW)
        cols = slice(g * GDIM, (g + 1) * GDIM)
        block = first_step * nblocks + b
        counted = jnp.logical_and(sum_id < block, sum_row < blocks_per_sum)[:, :, cols]
        carry = earlier[:, cols] + jnp.sum(
            jnp.sum(jnp.where(counted, bsum[:, :, cols], 0.0), axis=0), axis=0, keepdims=True
        )
        position = (
            sp * steps * tile + block * WINDOW
            + lax.broadcasted_iota(jnp.int32, (WINDOW, 1), 0) + 1
        )
        inv_pos = 1.0 / position.astype(F32)
        span = jnp.left_shift(jnp.int32(2), tp * groups + g)
        band = jnp.logical_and(dist >= 0, dist < span).astype(F32).astype(BF)
        sums = dot(jnp.concatenate([prefix, band], axis=0), rows[wr, cols])
        inv_count = 1.0 / jnp.minimum(position, span).astype(F32)
        pooled = (sums[WINDOW:] * inv_count - (sums[:WINDOW] + carry) * inv_pos).astype(BF)
        out[0, br, cols] = dot(pooled, wg[g]).astype(BF)

    units = [(b, kv) for b in range(nblocks) for kv in range(kvs)]
    pools = [(b, g) for b in range(nblocks) for g in range(groups)]
    scores = score(*units[0])
    pending = None
    for u, unit in enumerate(units):
        later = score(*units[u + 1]) if u + 1 < len(units) else None
        if pending is not None:
            collect(*pending)
        if u < len(pools):
            pool_block(*pools[u])
        pending = (*unit, *attend(*unit, scores))
        scores = later
    collect(*pending)
    for extra in pools[len(units) :]:
        pool_block(*extra)


def mix(mine, scal, q, kd, vt, pool, khalo, vhalo, phalo, totals, bsum, wg, sinks, *logs_in):
    length, qw = q.shape
    tile = 256
    per = tile // WINDOW
    steps = length // tile // 2
    pw = pool.shape[1]
    heads = sinks.shape[0]
    half = lambda s: s[0] if mine else 1 - s[0]
    cur = lambda i, s: half(s) * steps + i
    prev = lambda i, s: jnp.maximum(cur(i, s) * per - 1, 0)
    whole = lambda a: pl.BlockSpec(a.shape, lambda i, s: (0,) * a.ndim)
    return pl.pallas_call(
        functools.partial(mix_kernel, mine),
        grid_spec=pltpu.PrefetchScalarGridSpec(
            num_scalar_prefetch=1,
            grid=(steps,),
            in_specs=[
                pl.BlockSpec((tile, qw), lambda i, s: (cur(i, s), 0)),
                pl.BlockSpec((tile, kd.shape[1]), lambda i, s: (cur(i, s), 0)),
                pl.BlockSpec((WINDOW, kd.shape[1]), lambda i, s: (prev(i, s), 0)),
                pl.BlockSpec((vt.shape[0], tile), lambda i, s: (0, cur(i, s))),
                pl.BlockSpec((vt.shape[0], WINDOW), lambda i, s: (0, prev(i, s))),
                pl.BlockSpec((tile, pw), lambda i, s: (cur(i, s), 0)),
                pl.BlockSpec((WINDOW, pw), lambda i, s: (prev(i, s), 0)),
                whole(khalo), whole(vhalo), whole(phalo), whole(totals), whole(bsum), whole(wg),
                pl.BlockSpec(memory_space=pltpu.SMEM),
            ]
            + [pl.BlockSpec(memory_space=pl.ANY)] * len(logs_in),
            out_specs=[
                pl.BlockSpec((2, tile, qw), lambda i, s: (0, i, 0)),
                pl.BlockSpec((heads, tile), lambda i, s: (0, cur(i, s))),
            ],
        ),
        out_shape=[
            jax.ShapeDtypeStruct((2, length // 2, qw), BF),
            jax.ShapeDtypeStruct((heads, length), F32),
        ],
        input_output_aliases={15: 1} if logs_in else {},
        compiler_params=pltpu.CompilerParams(
            dimension_semantics=("arbitrary",), vmem_limit_bytes=VMEM
        ),
        cost_estimate=pl.CostEstimate(
            flops=length // 2 * 2 * qw * 1024, bytes_accessed=length * qw * 4,
            transcendentals=length // 2 * 1024,
        ),
        name="mix",
    )(scal, q, kd, kd, vt, vt, pool, pool, khalo, vhalo, phalo, totals, bsum, wg, sinks, *logs_in)


def share_kernel(count, kd, vt, pool, total, khalo, vhalo, phalo, totals, send, recv, tsend, trecv):
    me = lax.axis_index("sp")
    length = kd.shape[0]
    totals[...] = jnp.zeros_like(totals)
    barrier = pltpu.get_barrier_semaphore()
    for hop in range(1, count):
        pl.semaphore_signal(
            barrier, inc=1, device_id={"sp": lax.rem(me + hop, count)}, device_id_type=MESH
        )
    first = me == 0

    @pl.when(first)
    def _():
        khalo[...] = jnp.zeros_like(khalo)
        vhalo[...] = jnp.zeros_like(vhalo)
        phalo[...] = jnp.zeros_like(phalo)

    pl.semaphore_wait(barrier, count - 1)
    right = {"sp": lax.rem(me + 1, count)}
    pairs = (
        (kd.at[pl.ds(length - WINDOW, WINDOW), :], khalo),
        (vt.at[:, pl.ds(length - WINDOW, WINDOW)], vhalo),
        (pool.at[pl.ds(length - 16, 16), :], phalo),
    )
    halos = [
        pltpu.make_async_remote_copy(
            src_ref=src, dst_ref=dst, send_sem=send.at[j], recv_sem=recv.at[j],
            device_id=right, device_id_type=MESH,
        )
        for j, (src, dst) in enumerate(pairs)
    ]

    def sum_copy(hop):
        return pltpu.make_async_remote_copy(
            src_ref=total, dst_ref=totals.at[hop], send_sem=tsend.at[hop],
            recv_sem=trecv.at[hop], device_id={"sp": lax.rem(me + hop, count)},
            device_id_type=MESH,
        )

    @pl.when(me < count - 1)
    def _():
        for copy in halos:
            copy.start()

    for hop in range(1, count):

        @pl.when(me + hop < count)
        def _():
            sum_copy(hop).start()

    @pl.when(me > 0)
    def _():
        for copy in halos:
            copy.wait_recv()

    @pl.when(me < count - 1)
    def _():
        for copy in halos:
            copy.wait_send()

    for hop in range(1, count):

        @pl.when(me >= hop)
        def _():
            sum_copy(hop).wait_recv()

        @pl.when(me + hop < count)
        def _():
            sum_copy(hop).wait_send()


def share(kd, vt, pool, total):
    count = lax.axis_size("sp")
    vmem = pl.BlockSpec(memory_space=pltpu.VMEM)
    return pl.pallas_call(
        functools.partial(share_kernel, count),
        in_specs=[pl.BlockSpec(memory_space=pl.ANY)] * 3 + [vmem],
        out_specs=[vmem] * 4,
        out_shape=[
            jax.ShapeDtypeStruct((WINDOW, kd.shape[1]), BF),
            jax.ShapeDtypeStruct((vt.shape[0], WINDOW), BF),
            jax.ShapeDtypeStruct((16, pool.shape[1]), BF),
            jax.ShapeDtypeStruct((count, *total.shape), F32),
        ],
        scratch_shapes=[
            pltpu.SemaphoreType.DMA((3,)),
            pltpu.SemaphoreType.DMA((3,)),
            pltpu.SemaphoreType.DMA((count,)),
            pltpu.SemaphoreType.DMA((count,)),
        ],
        compiler_params=pltpu.CompilerParams(
            collective_id=0, has_side_effects=True, vmem_limit_bytes=VMEM
        ),
        name="share",
    )(kd, vt, pool, total)


def output_kernel(scal, own, other, w, out):
    tp = scal[0]
    width = own.shape[2]
    acc = None
    for kind in range(2):
        for x, who in ((own, tp), (other, 1 - tp)):
            start = pl.multiple_of((kind * 2 + who) * width, width)
            part = dot(x[kind], w[pl.ds(start, width), :])
            acc = part if acc is None else acc + part
    out[...] = acc.astype(BF)


def output(scal, own, other, w):
    rows, width = own.shape[1:]
    cols = w.shape[1]
    tile = 256
    return pl.pallas_call(
        output_kernel,
        grid_spec=pltpu.PrefetchScalarGridSpec(
            num_scalar_prefetch=1,
            grid=(cols // tile,),
            in_specs=[
                pl.BlockSpec(own.shape, lambda i, s: (0, 0, 0), pipeline_mode=pl.Buffered(1)),
                pl.BlockSpec(own.shape, lambda i, s: (0, 0, 0), pipeline_mode=pl.Buffered(1)),
                pl.BlockSpec((w.shape[0], tile), lambda i, s: (0, i)),
            ],
            out_specs=pl.BlockSpec((rows, tile), lambda i, s: (0, i)),
        ),
        out_shape=jax.ShapeDtypeStruct((rows, cols), BF),
        compiler_params=pltpu.CompilerParams(
            dimension_semantics=("arbitrary",), vmem_limit_bytes=VMEM
        ),
        cost_estimate=pl.CostEstimate(
            flops=2 * rows * w.shape[0] * cols, bytes_accessed=2 * w.size, transcendentals=0
        ),
        name="output",
    )(scal, own, other, w)


def body(tokens, norm_gain, w_query, w_key, w_value, w_pool, w_group, w_out, sinks):
    q, kd, vt, pool, bsum, total = project(
        tokens[0], norm_gain[None, :], w_query, w_key, w_value, w_pool
    )
    length = q.shape[0]
    halos = share(kd, vt, pool, total)
    per_sum = length // bsum.shape[0] // WINDOW
    scal = jnp.stack(
        [lax.axis_index("tp"), lax.axis_index("sp"), jnp.int32(length // 256), jnp.int32(per_sum)]
    ).astype(jnp.int32)
    shared = (scal, q, kd, vt, pool, *halos, bsum, w_group, sinks)
    theirs, logs = mix(False, *shared)
    other = lax.ppermute(theirs, "tp", [(0, 1), (1, 0)])
    own, logs = mix(True, *shared, logs)
    return (output(scal, own, other, w_out)[None], logs[None])


def solution(mesh):
    return jax.shard_map(
        body,
        mesh=mesh,
        in_specs=(
            P("fs", "sp", None),
            P(),
            P(None, "tp"),
            P(None, "tp"),
            P(None, "tp"),
            P(None, "tp"),
            P("tp", None, None),
            P(),
            P("tp"),
        ),
        out_specs=(P("fs", ("sp", "tp"), None), P("fs", "tp", "sp")),
        check_vma=False,
    )
```

profile of v0, /device:TPU:13, one launch (start us, length us, event | category | flops | bytes accessed | tf_op | source)
XLA Modules:
  0.0 67.7 jit_solution(1630744664818912907)
XLA Ops:
  0.6 0.6 pad_add_fusion.scal
  1.2 22.9 %project.1 = (bf16[2048,512]{1,0:T(8,128)(2,1)}, bf16[2048,256]{1,0:T(8,128)(2,1)}, bf16[128,2048]{1,0:T(8,128)(2,1)}, bf16[2048,512]{1,0:T(8,128)(2,1)}, f32[8,8,512]{2,1,0:T(8,128)}, /*index=5*/f32[1,512]{1,0:T(1,128)}) custom-call(bf16[2048,2048]{1,0:T(8,128)(2,1)} %bitcast.7, f32[1,2048]{1,0:T(1,128)} %bitcast.8, bf16[2048,512]{1,0:T(8,128)(2,1)} %wq.1, ...), custom_call_target="tpu_custom_call" | custom-call | flops 10737418240 | bytes 8388608 | tf_op jit(solution)/shard_map/project/pallas_call | solution.py:100
  24.2 7.8 %share.1 = (bf16[128,256]{1,0:T(8,128)(2,1)}, bf16[128,128]{1,0:T(8,128)(2,1)}, bf16[16,512]{1,0:T(8,128)(2,1)}, f32[4,1,512]{2,1,0:T(1,128)}) custom-call(bf16[2048,256]{1,0:T(8,128)(2,1)} %get-tuple-element.17.kd.kc.kp, bf16[128,2048]{1,0:T(8,128)(2,1)} %get-tuple-element.18.vt.vc.vp, bf16[2048,512]{1,0:T(8,128)(2,1)} %get-tuple-element.19.pool.pc.pp, ...), custom_call_target="tpu_custom_call" | custom-call | tf_op jit(solution)/shard_map/share/pallas_call | solution.py:377
  31.9 9.7 %mix.2 = (bf16[2,1024,512]{2,1,0:T(8,128)(2,1)}, f32[8,2048]{1,0:T(8,128)}) custom-call(s32[4]{0:T(128)} %pad_add_fusion.scal, bf16[2048,512]{1,0:T(8,128)(2,1)} %get-tuple-element.16.q, bf16[2048,256]{1,0:T(8,128)(2,1)} %get-tuple-element.17.kd.kc.kp, bf16[2048,256]{1,0:T(8,128)(2,1)} %get-tuple-element.17.kd.kc.kp, ...), custom_call_target="tpu_custom_call" | custom-call | flops 1073741824 | bytes 4194304 | tf_op jit(solution)/shard_map/mix/pallas_call | solution.py:265
  41.7 1.6 %collective-permute-start = (bf16[2,1024,512]{2,1,0:T(8,128)(2,1)}, bf16[2,1024,512]{2,1,0:T(8,128)(2,1)}, u32[]{:S(2)}, u32[]{:S(2)}) collective-permute-start(bf16[2,1024,512]{2,1,0:T(8,128)(2,1)} %get-tuple-element.28), channel_id=1, source_target_pairs={{0,1},{1,0},{2,3},{3,2},{4,5},{5,4},{6,7},{7,6},{8,9},{9,8},{10,11... | collective-permute-start | bytes 6291464 | tf_op jit(solution)/shard_map/ppermute | solution.py:451
  43.3 9.7 %mix.3 = (bf16[2,1024,512]{2,1,0:T(8,128)(2,1)}, f32[8,2048]{1,0:T(8,128)}) custom-call(s32[4]{0:T(128)} %pad_add_fusion.scal, bf16[2048,512]{1,0:T(8,128)(2,1)} %get-tuple-element.16.q, bf16[2048,256]{1,0:T(8,128)(2,1)} %get-tuple-element.17.kd.kc.kp, bf16[2048,256]{1,0:T(8,128)(2,1)} %get-tuple-element.17.kd.kc.kp, ...), custom_call_target="tpu_custom_call", output_to_operand_aliasing={{1}: (15, {})} | custom-call | flops 1073741824 | bytes 4194304 | tf_op jit(solution)/shard_map/mix/pallas_call | solution.py:265
  53.0 0.0 collective-permute-done.other
  53.0 14.7 %output.1 = bf16[1024,2048]{1,0:T(8,128)(2,1)} custom-call(s32[4]{0:T(128)} %pad_add_fusion.scal, bf16[2,1024,512]{2,1,0:T(8,128)(2,1)} %get-tuple-element.27.own, bf16[2,1024,512]{2,1,0:T(8,128)(2,1)} %collective-permute-done.other, bf16[2048,2048]{1,0:T(8,128)(2,1)} %w.1), custom_call_target="tpu_custom_call" | custom-call | flops 8589934592 | bytes 8388608 | tf_op jit(solution)/shard_map/output/pallas_call | solution.py:416
Async XLA Ops:
  41.7 11.3 %collective-permute-start = (bf16[2,1024,512]{2,1,0:T(8,128)(2,1)}, bf16[2,1024,512]{2,1,0:T(8,128)(2,1)}, u32[]{:S(2)}, u32[]{:S(2)}) collective-permute-start(bf16[2,1024,512]{2,1,0:T(8,128)(2,1)} %get-tuple-element.28), channel_id=1, source_target_pairs={{0,1},{1,0},{2,3},{3,2},{4,5},{5,4},{6,7},{7,6},{8,9},{9,8},{10,11... | collective-permute-start | bytes 6291464 | tf_op jit(solution)/shard_map/ppermute | solution.py:451
where the time goes:
time: 68.2 us; the launch traced here: 67.7 us
  Pallas kernels  64.8 us (95%)
  starting transfers between devices  1.64 us (2%)
    pallas_call x1, Pallas kernels, project(): pl.pallas_call(functools.partial(project_kernel, steps), grid=(steps + 1,...  22.9 us
    pallas_call x2, Pallas kernels, mix(): pl.pallas_call(functools.partial(mix_kernel, mine), grid_spec=pltpu.Prefe...  19.4 us
    pallas_call x1, Pallas kernels, output(): pl.pallas_call(output_kernel, grid_spec=pltpu.PrefetchScalarGridSpec(num_...  14.7 us
    pallas_call x1, Pallas kernels, share(): pl.pallas_call(functools.partial(share_kernel, count), in_specs=[pl.Block...  7.77 us
    ppermute x1, starting transfers between devices, body(): other = lax.ppermute(theirs, 'tp', [(0, 1), (1, 0)])  1.64 us
  transfers between devices with their start and end apart: 1, of which 0 were waited for; matrix products, arithmetic and copies ran while one was open for 0% of the time, Pallas kernels for 14%

commit v1 on v0

--- a/solution.py
+++ b/solution.py
@@ -11,6 +11,7 @@
 GDIM = 256
 WINDOW = 128
 LN_EPS = 1e-05
+SUB = 256
 VMEM = 63 * 2**20
 MESH = pl.DeviceIdType.MESH
 BF = jnp.bfloat16
@@ -22,94 +23,62 @@
     return lax.dot_general(a, b, (dims, ((), ())), preferred_element_type=F32)
 
 
-def normalize(tok, gain, normed):
+def project_kernel(subs, tok, gain, wq, wk, wv, wp, q, kd, vt, pool, bsum, total):
+    step = pl.program_id(0)
     width = tok.shape[1]
-
-    def chunk(j):
-        rows = slice(j * 64, (j + 1) * 64)
+    rows_sums = []
+    for s in range(subs):
+        rows = slice(s * SUB, (s + 1) * SUB)
         x = tok[rows, :].astype(F32)
         centered = x - jnp.sum(x, axis=-1, keepdims=True) * (1.0 / width)
         variance = jnp.sum(centered * centered, axis=-1, keepdims=True) * (1.0 / width)
-        normed[rows, :] = (centered * lax.rsqrt(variance + LN_EPS) * gain[...]).astype(BF)
-
-    return [functools.partial(chunk, j) for j in range(tok.shape[0] // 64)]
-
-
-def multiply(normed, wq, wk, wv, wp, q, kd, vt, pool, bsum, total, step):
-    def do_q():
-        q[...] = (dot(normed[...], wq[...]) * HEAD_SIZE**-0.5).astype(BF)
-
-    def do_k():
-        k = dot(normed[...], wk[...])
+        normed = (centered * lax.rsqrt(variance + LN_EPS) * gain[...]).astype(BF)
+        q[rows, :] = (dot(normed, wq[...]) * HEAD_SIZE**-0.5).astype(BF)
+        k = dot(normed, wk[...])
         rolled = pltpu.roll(k, HEAD_SIZE, 1)
         low = lax.broadcasted_iota(jnp.int32, k.shape, 1) < HEAD_SIZE
-        kd[:, :WINDOW] = jnp.where(low, k, rolled).astype(BF)
-        kd[:, WINDOW:] = jnp.where(low, rolled, k).astype(BF)
-
-    def do_v():
-        vt[...] = dot(normed[...], wv[...]).T.astype(BF)
-
-    def do_p():
-        p = dot(normed[...], wp[...]).astype(BF)
-        pool[...] = p
+        kd[rows, :WINDOW] = jnp.where(low, k, rolled).astype(BF)
+        kd[rows, WINDOW:] = jnp.where(low, rolled, k).astype(BF)
+        vt[:, rows] = dot(normed, wv[...]).T.astype(BF)
+        p = dot(normed, wp[...]).astype(BF)
+        pool[rows, :] = p
         pf = p.astype(F32)
-        sums = [
-            jnp.sum(pf[b * WINDOW : (b + 1) * WINDOW], axis=0, keepdims=True)
-            for b in range(p.shape[0] // WINDOW)
-        ]
-        tile_sum = functools.reduce(lambda a, b: a + b, sums)
-        pad = jnp.zeros((8 - len(sums), pool.shape[1]), F32)
-        bsum[0] = jnp.concatenate(sums + [pad], axis=0)
-        total[...] = jnp.where(step > 1, total[...], 0.0) + tile_sum
-
-    return [do_q, do_k, do_v, do_p]
-
-
-def project_kernel(steps, tok, gain, wq, wk, wv, wp, q, kd, vt, pool, bsum, total, even, odd):
-    step = pl.program_id(0)
-    rest = (wq, wk, wv, wp, q, kd, vt, pool, bsum, total, step)
+        for b in range(SUB // WINDOW):
+            rows_sums.append(
+                jnp.sum(pf[b * WINDOW : (b + 1) * WINDOW], axis=0, keepdims=True)
+            )
+    tile_sum = functools.reduce(lambda a, b: a + b, rows_sums)
+    pad = jnp.zeros((8 - len(rows_sums), pool.shape[1]), F32)
+    bsum[0] = jnp.concatenate(rows_sums + [pad], axis=0)
 
     @pl.when(step == 0)
     def _():
-        for f in normalize(tok, gain, even):
-            f()
-
-    for parity in range(2):
-        here, before = (even, odd) if parity == 0 else (odd, even)
-
-        @pl.when((step > 0) & (step < steps) & (step % 2 == parity))
-        def _():
-            norms, mults = normalize(tok, gain, here), multiply(before, *rest)
-            for n, m in zip(norms, mults):
-                n()
-                m()
-
-    @pl.when(step == steps)
-    def _():
-        for f in multiply(odd if steps % 2 == 0 else even, *rest):
-            f()
+        total[...] = tile_sum
+
+    @pl.when(step > 0)
+    def _():
+        total[...] += tile_sum
 
 
 def project(tokens, gain, wq, wk, wv, wp):
     length, width = tokens.shape
-    tile = 256
+    tile = 512
     steps = length // tile
-    late = lambda i: jnp.maximum(i - 1, 0)
     qw, kw, pw = wq.shape[1], wk.shape[1], wp.shape[1]
     whole = lambda a: pl.BlockSpec(a.shape, lambda i: (0, 0), pipeline_mode=pl.Buffered(1))
     return pl.pallas_call(
-        functools.partial(project_kernel, steps),
-        grid=(steps + 1,),
+        functools.partial(project_kernel, tile // SUB),
+        grid=(steps,),
         in_specs=[
-            pl.BlockSpec((tile, width), lambda i: (jnp.minimum(i, steps - 1), 0)),
+            pl.BlockSpec((tile, width), lambda i: (i, 0)),
             whole(gain), whole(wq), whole(wk), whole(wv), whole(wp),
         ],
         out_specs=[
-            pl.BlockSpec((tile, qw), lambda i: (late(i), 0)),
-            pl.BlockSpec((tile, 2 * kw), lambda i: (late(i), 0)),
-            pl.BlockSpec((kw, tile), lambda i: (0, late(i))),
-            pl.BlockSpec((tile, pw), lambda i: (late(i), 0)),
-            pl.BlockSpec((1, 8, pw), lambda i: (late(i), 0, 0)),
+            pl.BlockSpec((tile, qw), lambda i: (i, 0)),
+            pl.BlockSpec((tile, 2 * kw), lambda i: (i, 0)),
+            pl.BlockSpec((kw, tile), lambda i: (0, i)),
+            pl.BlockSpec((tile, pw), lambda i: (i, 0)),
+            pl.BlockSpec((1, 8, pw), lambda i: (i, 0, 0)),
             pl.BlockSpec((1, pw), lambda i: (0, 0)),
         ],
         out_shape=[
@@ -120,7 +89,6 @@
             jax.ShapeDtypeStruct((steps, 8, pw), F32),
             jax.ShapeDtypeStruct((1, pw), F32),
         ],
-        scratch_shapes=[pltpu.VMEM((tile, width), BF)] * 2,
         compiler_params=pltpu.CompilerParams(
             dimension_semantics=("arbitrary",), vmem_limit_bytes=VMEM
         ),
@@ -397,43 +365,52 @@
     )(kd, vt, pool, total)
 
 
-def output_kernel(scal, own, other, w, out):
-    tp = scal[0]
+def output_kernel(own, other, w, out, joined, sems):
     width = own.shape[2]
-    acc = None
-    for kind in range(2):
-        for x, who in ((own, tp), (other, 1 - tp)):
-            start = pl.multiple_of((kind * 2 + who) * width, width)
-            part = dot(x[kind], w[pl.ds(start, width), :])
-            acc = part if acc is None else acc + part
-    out[...] = acc.astype(BF)
-
-
-def output(scal, own, other, w):
-    rows, width = own.shape[1:]
-    cols = w.shape[1]
-    tile = 256
+
+    @pl.when(pl.program_id(0) == 0)
+    def _():
+        tp = lax.axis_index("tp")
+        copies = []
+        for kind in range(2):
+            for j, (x, who) in enumerate(((own, tp), (other, 1 - tp))):
+                start = pl.multiple_of((kind * 2 + who) * width, width)
+                copies.append(
+                    pltpu.make_async_copy(
+                        x.at[kind], joined.at[:, pl.ds(start, width)], sems.at[kind * 2 + j]
+                    )
+                )
+        for copy in copies:
+            copy.start()
+        for copy in copies:
+            copy.wait()
+
+    out[...] = dot(joined[...], w[...]).astype(BF)
+
+
+def output(own, other, w):
+    rows = own.shape[1]
+    depth, cols = w.shape
+    tile = 512
     return pl.pallas_call(
         output_kernel,
-        grid_spec=pltpu.PrefetchScalarGridSpec(
-            num_scalar_prefetch=1,
-            grid=(cols // tile,),
-            in_specs=[
-                pl.BlockSpec(own.shape, lambda i, s: (0, 0, 0), pipeline_mode=pl.Buffered(1)),
-                pl.BlockSpec(own.shape, lambda i, s: (0, 0, 0), pipeline_mode=pl.Buffered(1)),
-                pl.BlockSpec((w.shape[0], tile), lambda i, s: (0, i)),
-            ],
-            out_specs=pl.BlockSpec((rows, tile), lambda i, s: (0, i)),
-        ),
+        grid=(cols // tile,),
+        in_specs=[
+            pl.BlockSpec(memory_space=pl.ANY),
+            pl.BlockSpec(memory_space=pl.ANY),
+            pl.BlockSpec((depth, tile), lambda i: (0, i)),
+        ],
+        out_specs=pl.BlockSpec((rows, tile), lambda i: (0, i)),
         out_shape=jax.ShapeDtypeStruct((rows, cols), BF),
+        scratch_shapes=[pltpu.VMEM((rows, depth), BF), pltpu.SemaphoreType.DMA((4,))],
         compiler_params=pltpu.CompilerParams(
             dimension_semantics=("arbitrary",), vmem_limit_bytes=VMEM
         ),
         cost_estimate=pl.CostEstimate(
-            flops=2 * rows * w.shape[0] * cols, bytes_accessed=2 * w.size, transcendentals=0
+            flops=2 * rows * depth * cols, bytes_accessed=2 * w.size, transcendentals=0
         ),
         name="output",
-    )(scal, own, other, w)
+    )(own, other, w)
 
 
 def body(tokens, norm_gain, w_query, w_key, w_value, w_pool, w_group, w_out, sinks):
@@ -450,7 +427,7 @@
     theirs, logs = mix(False, *shared)
     other = lax.ppermute(theirs, "tp", [(0, 1), (1, 0)])
     own, logs = mix(True, *shared, logs)
-    return (output(scal, own, other, w_out)[None], logs[None])
+    return (output(own, other, w_out)[None], logs[None])
 
 
 def solution(mesh):

time: 68.2 us -> 66 us (0.968)
  Pallas kernels: 64.8 us -> 62.8 us
    pallas_call x2, Pallas kernels: 37.6 us -> 35.8 us  [the longest x1 21.4 us: project(): pl.pallas_call(functools.partial(project_kernel, tile // SUB), grid=(step...]
  transfers between devices with their start and end apart: 1 -> 1, of which waited for: 0 -> 0; matrix products, arithmetic and copies ran while one was open for 0% -> 0% of each run, Pallas kernels for 14% -> 15%
where the time goes in v1:
time: 66 us; the launch traced here: 65.7 us
  Pallas kernels  62.8 us (95%)
  starting transfers between devices  1.67 us (3%)
  between operations  0.66 us (1%)
    pallas_call x1, Pallas kernels, project(): pl.pallas_call(functools.partial(project_kernel, tile // SUB), grid=(step...  21.4 us
    pallas_call x2, Pallas kernels, mix(): pl.pallas_call(functools.partial(mix_kernel, mine), grid_spec=pltpu.Prefe...  19.3 us
    pallas_call x1, Pallas kernels, output(): pl.pallas_call(output_kernel, grid=(cols // tile,), in_specs=[pl.BlockSpe...  14.3 us
    pallas_call x1, Pallas kernels, share(): pl.pallas_call(functools.partial(share_kernel, count), in_specs=[pl.Block...  7.74 us
    ppermute x1, starting transfers between devices, body(): other = lax.ppermute(theirs, 'tp', [(0, 1), (1, 0)])  1.67 us
  transfers between devices with their start and end apart: 1, of which 0 were waited for; matrix products, arithmetic and copies ran while one was open for 0% of the time, Pallas kernels for 15%

profile of v1, /device:TPU:13, one launch (start us, length us, event | category | flops | bytes accessed | tf_op | source)
XLA Modules:
  0.0 65.7 jit_solution(4744575068777697888)
XLA Ops:
  0.6 0.6 pad_add_fusion.scal
  1.2 21.4 %project.1 = (bf16[2048,512]{1,0:T(8,128)(2,1)}, bf16[2048,256]{1,0:T(8,128)(2,1)}, bf16[128,2048]{1,0:T(8,128)(2,1)}, bf16[2048,512]{1,0:T(8,128)(2,1)}, f32[4,8,512]{2,1,0:T(8,128)}, /*index=5*/f32[1,512]{1,0:T(1,128)}) custom-call(bf16[2048,2048]{1,0:T(8,128)(2,1)} %bitcast.7, f32[1,2048]{1,0:T(1,128)} %bitcast.8, bf16[2048,512]{1,0:T(8,128)(2,1)} %wq.1, ...), custom_call_target="tpu_custom_call" | custom-call | flops 10737418240 | bytes 8388608 | tf_op jit(solution)/shard_map/project/pallas_call | solution.py:69
  22.7 7.7 %share.1 = (bf16[128,256]{1,0:T(8,128)(2,1)}, bf16[128,128]{1,0:T(8,128)(2,1)}, bf16[16,512]{1,0:T(8,128)(2,1)}, f32[4,1,512]{2,1,0:T(1,128)}) custom-call(bf16[2048,256]{1,0:T(8,128)(2,1)} %get-tuple-element.17.kd.kc.kp, bf16[128,2048]{1,0:T(8,128)(2,1)} %get-tuple-element.18.vt.vc.vp, bf16[2048,512]{1,0:T(8,128)(2,1)} %get-tuple-element.19.pool.pc.pp, ...), custom_call_target="tpu_custom_call" | custom-call | tf_op jit(solution)/shard_map/share/pallas_call | solution.py:345
  30.4 9.7 %mix.2 = (bf16[2,1024,512]{2,1,0:T(8,128)(2,1)}, f32[8,2048]{1,0:T(8,128)}) custom-call(s32[4]{0:T(128)} %pad_add_fusion.scal, bf16[2048,512]{1,0:T(8,128)(2,1)} %get-tuple-element.16.q, bf16[2048,256]{1,0:T(8,128)(2,1)} %get-tuple-element.17.kd.kc.kp, bf16[2048,256]{1,0:T(8,128)(2,1)} %get-tuple-element.17.kd.kc.kp, ...), custom_call_target="tpu_custom_call" | custom-call | flops 1073741824 | bytes 4194304 | tf_op jit(solution)/shard_map/mix/pallas_call | solution.py:233
  40.1 1.7 %collective-permute-start = (bf16[2,1024,512]{2,1,0:T(8,128)(2,1)}, bf16[2,1024,512]{2,1,0:T(8,128)(2,1)}, u32[]{:S(2)}, u32[]{:S(2)}) collective-permute-start(bf16[2,1024,512]{2,1,0:T(8,128)(2,1)} %get-tuple-element.28), channel_id=1, source_target_pairs={{0,1},{1,0},{2,3},{3,2},{4,5},{5,4},{6,7},{7,6},{8,9},{9,8},{10,11... | collective-permute-start | bytes 6291464 | tf_op jit(solution)/shard_map/ppermute | solution.py:428
  41.8 9.6 %mix.3 = (bf16[2,1024,512]{2,1,0:T(8,128)(2,1)}, f32[8,2048]{1,0:T(8,128)}) custom-call(s32[4]{0:T(128)} %pad_add_fusion.scal, bf16[2048,512]{1,0:T(8,128)(2,1)} %get-tuple-element.16.q, bf16[2048,256]{1,0:T(8,128)(2,1)} %get-tuple-element.17.kd.kc.kp, bf16[2048,256]{1,0:T(8,128)(2,1)} %get-tuple-element.17.kd.kc.kp, ...), custom_call_target="tpu_custom_call", output_to_operand_aliasing={{1}: (15, {})} | custom-call | flops 1073741824 | bytes 4194304 | tf_op jit(solution)/shard_map/mix/pallas_call | solution.py:233
  51.4 0.0 collective-permute-done.other
  51.4 14.3 %output.1 = bf16[1024,2048]{1,0:T(8,128)(2,1)} custom-call(bf16[2,1024,512]{2,1,0:T(8,128)(2,1)} %get-tuple-element.27.own, bf16[2,1024,512]{2,1,0:T(8,128)(2,1)} %collective-permute-done.other, bf16[2048,2048]{1,0:T(8,128)(2,1)} %w.1), custom_call_target="tpu_custom_call" | custom-call | flops 8589934592 | bytes 8388608 | tf_op jit(solution)/shard_map/output/pallas_call | solution.py:395
Async XLA Ops:
  40.1 11.3 %collective-permute-start = (bf16[2,1024,512]{2,1,0:T(8,128)(2,1)}, bf16[2,1024,512]{2,1,0:T(8,128)(2,1)}, u32[]{:S(2)}, u32[]{:S(2)}) collective-permute-start(bf16[2,1024,512]{2,1,0:T(8,128)(2,1)} %get-tuple-element.28), channel_id=1, source_target_pairs={{0,1},{1,0},{2,3},{3,2},{4,5},{5,4},{6,7},{7,6},{8,9},{9,8},{10,11... | collective-permute-start | bytes 6291464 | tf_op jit(solution)/shard_map/ppermute | solution.py:428
